TPU v7x, 32 devices: a whole 2x2x4 slice. The times are simulated.
32 devices in a mesh: ep: 8 (over z, core), tp: 4 (over y, x).
Axes of the slice: x: 2, y: 2, z: 4, core: 2. Of those that a mesh axis runs over, the one named last changes fastest.
Arguments:
- tokens: bfloat16 [4096, 2048], P(('ep', 'tp')), may hold values from -6 to 6
- norm_gain: float32 [2048], replicated, may hold values from 0.1 to 1.9
- expert_ids: int32 [4096, 2], P(('ep', 'tp')), may hold values from 0 to 7, all different within a row; in each aligned block of 128 rows (0 to 127, 128 to 255, ...) at most 64 rows name the same one
- gate_weights: float32 [4096, 2], P(('ep', 'tp')), may hold values from 0.2 to 1.6
- expert_gate: bfloat16 [8, 512, 2048], P('ep', 'tp'), may hold values from -0.125 to 0.125
- expert_up: bfloat16 [8, 512, 2048], P('ep', 'tp'), may hold values from -0.125 to 0.125
- expert_down: bfloat16 [8, 512, 2048], P('ep', 'tp'), may hold values from -0.25 to 0.25
- shared_gate: bfloat16 [512, 2048], P('tp'), may hold values from -0.125 to 0.125
- shared_up: bfloat16 [512, 2048], P('tp'), may hold values from -0.125 to 0.125
- shared_down: bfloat16 [512, 2048], P('tp'), may hold values from -0.25 to 0.25
Outputs:
- mixed: bfloat16 [4096, 2048], P(('ep', 'tp'))
Inputs may be any that keep to these rules, and one draw needn't show every extreme that they name: `expert_ids`: each row names 2 different experts. Within the rows of one device no expert is named by more than 64 rows, and in every draw some expert is named by exactly 64 rows of some device.
All inputs are finite; a program needn't handle non-finite values.
Results may differ from a plain program's by a relative error of at most 0.0068.
Values may be sent and summed in bfloat16 or wider, within the bound.
A program may use at most 64 MiB of HBM per device.

v0:
```python
import functools
import math

import jax
import jax.numpy as jnp
from jax import lax
from jax.experimental import pallas as pl
from jax.experimental.pallas import tpu as pltpu
from jax.sharding import PartitionSpec as P

EPS = 1e-06
MESH = pl.DeviceIdType.MESH
NT = (((1,), (1,)), ((), ()))
F32 = jnp.float32
BF16 = jnp.bfloat16
CHUNKS = 4


def remote(src, dst, send, recv, where):
    return pltpu.make_async_remote_copy(
        src_ref=src, dst_ref=dst, send_sem=send, recv_sem=recv, device_id=where, device_id_type=MESH
    )


def kernel(
    ep, tp, xs, ys, cap,
    tok_ref, gain_ref, route_ref, eg, eu, ed, sg, su, sd, out_ref,
    wts, swts, normed, mix, spread, pick, tokens, arrived, hidden, results, returned,
    s1, r1, s2, r2, s3, r3, sp, rp, st, rt, sd2, rd2, sb, rb,
):
    e = lax.axis_index("ep")
    t = lax.axis_index("tp")
    y, x = t // xs, t % xs
    z, core = e // 2, e % 2
    nz = ep // 2
    partner = e + 1 - 2 * core
    rows, d_model = tok_ref.shape
    own_rows = eg.shape[0]
    srows = sg.shape[0] // 2
    slots = ep * cap
    piece = d_model // CHUNKS
    last = 2 + CHUNKS

    def at(dy, dx):
        return lax.rem(y + dy, ys) * xs + lax.rem(x + dx, xs)

    row_peers = [at(0, i) for i in range(1, xs)]
    col_peers = [at(i, 0) for i in range(1, ys)]
    diagonal = [at(i, j) for i in range(1, ys) for j in range(1, xs)]
    if ep & (ep - 1) == 0:
        bits = [1 << b for b in range(ep.bit_length() - 1)]
        ep_peers = [sum((e // b + i // b) % 2 * b for b in bits) for i in range(ep - 1, 0, -1)]
    else:
        ep_peers = [lax.rem(e + i, ep) for i in range(1, ep)]

    barrier = pltpu.get_barrier_semaphore()
    for p in row_peers + col_peers:
        pl.semaphore_signal(barrier, inc=1, device_id={"tp": p}, device_id_type=MESH)
    for p in ep_peers:
        pl.semaphore_signal(barrier, inc=1, device_id={"ep": p}, device_id_type=MESH)
    pl.semaphore_wait(barrier, len(row_peers) + len(col_peers) + len(ep_peers))

    sends = []
    mine = pl.ds(pl.multiple_of(core * srows, srows), srows)

    def columns(a):
        return ((a - 2) * piece, piece) if 2 <= a < last else (0, d_model)

    def view(a, owner, start, size):
        cols = pl.ds(start, size)
        if a < last:
            return wts.at[min(a, 2), owner, :, cols]
        return swts.at[a - last, core, owner, :, cols]

    def block(a, owner):
        return view(a, owner, *columns(a))

    def part(a, owner, h):
        start, size = columns(a)
        return view(a, owner, start + h * (size // 2), size // 2)

    def own(a):
        if a < last:
            start, size = columns(a)
            return (eg, eu, ed)[min(a, 2)].at[:, pl.ds(start, size)]
        return (sg, su, sd)[a - last].at[mine]

    def first(a):
        for j, p in enumerate(row_peers + col_peers):
            c = remote(own(a), block(a, t), s1.at[a, j], r1.at[a, t], {"tp": p})
            c.start()
            sends.append(c)

    def first_done(a):
        for q in row_peers + col_peers:
            remote(block(a, q), block(a, q), s1.at[a, 0], r1.at[a, q], {"tp": q}).wait_recv()

    def second(a):
        for h, (owners, peers) in enumerate(((col_peers, row_peers), (row_peers, col_peers))):
            for i, q in enumerate(owners):
                for j, p in enumerate(peers):
                    c = remote(part(a, q, h), part(a, q, h), s2.at[a, h, i, j], r2.at[a, h, q], {"tp": p})
                    c.start()
                    sends.append(c)

    def second_done(a):
        for q in diagonal:
            for h in range(2):
                remote(part(a, q, h), part(a, q, h), s2.at[a, h, 0, 0], r2.at[a, h, q], {"tp": q}).wait_recv()

    def hop(src, sign, source):
        slot = 2 * src + core
        d = 0 if sign > 0 else 1
        return remote(source, tokens.at[slot], st.at[d, src], rt.at[src], {"ep": e + 2 * sign})

    def over(src, source):
        slot = 2 * src + core
        return remote(source, tokens.at[slot], sd2.at[src], rd2.at[src], {"ep": partner})

    def from_partner(src):
        slot = 2 * src + 1 - core
        return remote(tokens.at[slot], tokens.at[slot], sd2.at[src], rd2.at[src], {"ep": partner})

    def pack(src_ep, source):
        raw = jnp.dot(pick[src_ep], source[...], preferred_element_type=F32)
        scale = lax.rsqrt(jnp.mean(raw * raw, axis=-1, keepdims=True) + EPS)
        arrived[src_ep] = (raw * scale * gain_ref[...]).astype(BF16)

    def pick_done(src_ep):
        remote(pick.at[src_ep], pick.at[src_ep], sp.at[0], rp.at[src_ep], {"ep": partner}).wait_recv()

    first(0)

    @pl.when(z + 1 < nz)
    def _():
        hop(z, 1, tok_ref).start()

    @pl.when(z > 0)
    def _():
        hop(z, -1, tok_ref).start()

    over(z, tok_ref).start()
    first(1)

    chosen = route_ref.shape[1] // 2
    ids = route_ref[:, :chosen]
    labels = lax.broadcasted_iota(jnp.int32, (rows, ep), 1).astype(F32)
    one_hot = [(ids[:, k : k + 1] == labels).astype(F32) for k in range(chosen)]
    hits = sum(one_hot[1:], one_hot[0])
    lower = (
        lax.broadcasted_iota(jnp.int32, (rows, rows), 1) < lax.broadcasted_iota(jnp.int32, (rows, rows), 0)
    ).astype(F32).astype(BF16)
    before = jnp.dot(lower, hits.astype(BF16), preferred_element_type=F32)
    slot_ids = lax.broadcasted_iota(jnp.int32, (rows, slots), 1).astype(F32)
    weights = jnp.zeros((rows, slots), F32)
    placing = jnp.zeros((rows, slots), F32)
    for k in range(chosen):
        place = ids[:, k : k + 1] * cap + jnp.sum(before * one_hot[k], axis=1, keepdims=True)
        hit = (place == slot_ids).astype(F32)
        placing = placing + hit
        weights = weights + route_ref[:, chosen + k : chosen + k + 1] * hit
    spread[...] = placing.T.astype(BF16).reshape(ep, cap, rows)
    high = weights.astype(BF16)
    mix[0] = high
    mix[1] = (weights - high.astype(F32)).astype(BF16)
    for j, p in enumerate(ep_peers):
        c = remote(spread.at[p], pick.at[e], sp.at[j], rp.at[e], {"ep": p})
        c.start()
        sends.append(c)
    pick[e] = spread[e]
    tok = tok_ref[...].astype(F32)
    nrm = tok * lax.rsqrt(jnp.mean(tok * tok, axis=-1, keepdims=True) + EPS) * gain_ref[...]
    normed[...] = nrm.astype(BF16)
    for a, ref in enumerate((eg, eu, ed)):
        wts[a, t] = ref[...]
    for a, ref in enumerate((sg, su, sd)):
        swts[a, core, t] = ref[mine, :]
    pack(e, tok_ref)
    for p in ep_peers:
        pick_done(p)
    from_partner(z).wait_recv()
    pack(partner, tokens.at[partner])

    first_done(0)
    second(0)

    def packs(step):
        for sign in (1, -1):
            src = z - sign * (step + 1)
            there = (src >= 0) if sign > 0 else (src < nz)

            @pl.when(there)
            def _():
                pack(2 * src + core, tokens.at[2 * src + core])
                from_partner(src).wait_recv()
                pack(2 * src + 1 - core, tokens.at[2 * src + 1 - core])

    for step in range(nz - 1):
        for sign in (1, -1):
            src = z - sign * (step + 1)
            there = (src >= 0) if sign > 0 else (src < nz)
            on = (z + 1 < nz) if sign > 0 else (z > 0)

            @pl.when(there)
            def _():
                here = tokens.at[2 * src + core]
                hop(src, sign, here).wait_recv()

                @pl.when(on)
                def _():
                    hop(src, sign, here).start()

                over(src, here).start()

        if step == 0:
            packs(0)
            first_done(1)
            second(1)
            first(2)
        else:
            packs(step)
    if nz == 1:
        first_done(1)
        second(1)
        first(2)

    first_done(2)
    second(2)
    first(3)
    first(4)
    second_done(0)
    second_done(1)
    per = max(1, min(tp, 256 // own_rows))
    width = per * own_rows
    for c in range(tp // per):
        held = arrived[...].reshape(slots, d_model)
        gate = lax.dot_general(held, wts[0, c * per : (c + 1) * per].reshape(width, d_model), NT, preferred_element_type=F32)
        up = lax.dot_general(held, wts[1, c * per : (c + 1) * per].reshape(width, d_model), NT, preferred_element_type=F32)
        hidden[:, c * width : (c + 1) * width] = (gate * (1.0 / (1.0 + jnp.exp(-gate))) * up).astype(BF16)

    def back(n, p, j):
        cols = pl.ds(n * piece, piece)
        return remote(results.at[p, :, cols], returned.at[e, :, cols], sb.at[n, j], rb.at[n, e], {"ep": p})

    total = last + 3
    for n in range(CHUNKS):
        second_done(n + 2)
        cols = slice(n * piece, (n + 1) * piece)
        down = wts[2, :, :, cols].reshape(tp * own_rows, piece)
        o = jnp.dot(hidden[...], down, preferred_element_type=F32).astype(BF16)
        results[:, :, cols] = o.reshape(ep, cap, piece)
        for j, p in enumerate(ep_peers):
            c = back(n, p, j)
            c.start()
            sends.append(c)
        returned[e, :, cols] = results[e, :, cols]
        first_done(n + 3)
        second(n + 3)
        if n + 5 < total:
            first(n + 5)

    def swap(a):
        return remote(swts.at[a, core], swts.at[a, core], s3.at[a], r3.at[a], {"ep": partner})

    for a in range(1, 3):
        first_done(last + a)
        second(last + a)
    for a in range(3):
        second_done(last + a)
        c = swap(a)
        c.start()
        sends.append(c)
    for a in range(3):
        other = swts.at[a, 1 - core]
        remote(other, other, s3.at[a], r3.at[a], {"ep": partner}).wait_recv()
    sall = 2 * tp * srows
    gate = lax.dot_general(normed[...], swts[0].reshape(sall, d_model), NT, preferred_element_type=F32)
    up = lax.dot_general(normed[...], swts[1].reshape(sall, d_model), NT, preferred_element_type=F32)
    shared_hidden = (gate * (1.0 / (1.0 + jnp.exp(-gate))) * up).astype(BF16)

    for n in range(CHUNKS):
        cols = slice(n * piece, (n + 1) * piece)
        sdown = swts[2, :, :, :, cols].reshape(sall, piece)
        sum_shared = jnp.dot(shared_hidden, sdown, preferred_element_type=F32)
        for p in ep_peers:
            c = returned.at[p, :, pl.ds(n * piece, piece)]
            remote(c, c, sb.at[0, 0], rb.at[n, p], {"ep": p}).wait_recv()
        given = returned[:, :, cols].reshape(slots, piece)
        routed = jnp.dot(mix[0], given, preferred_element_type=F32)
        routed = routed + jnp.dot(mix[1], given, preferred_element_type=F32)
        out_ref[:, cols] = (routed + sum_shared).astype(BF16)
    for c in sends:
        c.wait_send()

    over(z, tok_ref).wait_send()

    @pl.when(z + 1 < nz)
    def _():
        hop(z, 1, tok_ref).wait_send()

    @pl.when(z > 0)
    def _():
        hop(z, -1, tok_ref).wait_send()

    for step in range(nz - 1):
        for sign in (1, -1):
            src = z - sign * (step + 1)
            there = (src >= 0) if sign > 0 else (src < nz)
            on = (z + 1 < nz) if sign > 0 else (z > 0)

            @pl.when(there)
            def _():
                here = tokens.at[2 * src + core]
                over(src, here).wait_send()

                @pl.when(on)
                def _():
                    hop(src, sign, here).wait_send()


def body(ep, tp, tokens, norm_gain, expert_ids, gate_weights, eg, eu, ed, sg, su, sd):
    rows, d_model = tokens.shape
    cap = 2 * rows * expert_ids.shape[1] // ep
    side = math.isqrt(tp)
    xs = side if side * side == tp else tp
    ys = tp // xs
    own_rows = eg.shape[1]
    srows = sg.shape[0] // 2
    near = xs + ys - 2
    route = jnp.concatenate([expert_ids.astype(F32), gate_weights], axis=1)
    far = max(xs, ys)
    moves = 2 + CHUNKS + 3
    dma = pltpu.SemaphoreType.DMA
    vm = pl.BlockSpec(memory_space=pltpu.VMEM)
    return pl.pallas_call(
        functools.partial(kernel, ep, tp, xs, ys, cap),
        out_shape=jax.ShapeDtypeStruct((rows, d_model), BF16),
        in_specs=[vm] * 9,
        out_specs=vm,
        scratch_shapes=[
            pltpu.VMEM((3, tp, own_rows, d_model), BF16),
            pltpu.VMEM((3, 2, tp, srows, d_model), BF16),
            pltpu.VMEM((rows, d_model), BF16),
            pltpu.VMEM((2, rows, ep * cap), BF16),
            pltpu.VMEM((ep, cap, rows), BF16),
            pltpu.VMEM((ep, cap, rows), BF16),
            pltpu.VMEM((ep, rows, d_model), BF16),
            pltpu.VMEM((ep, cap, d_model), BF16),
            pltpu.VMEM((ep * cap, tp * own_rows), BF16),
            pltpu.VMEM((ep, cap, d_model), BF16),
            pltpu.VMEM((ep, cap, d_model), BF16),
            dma((moves, near)),
            dma((moves, tp)),
            dma((moves, 2, far, far)),
            dma((moves, 2, tp)),
            dma((3,)),
            dma((3,)),
            dma((ep,)),
            dma((ep,)),
            dma((2, ep // 2)),
            dma((ep // 2,)),
            dma((ep // 2,)),
            dma((ep // 2,)),
            dma((CHUNKS, ep)),
            dma((CHUNKS, ep)),
        ],
        compiler_params=pltpu.CompilerParams(
            collective_id=0, has_side_effects=True, vmem_limit_bytes=62 * 1024 * 1024
        ),
        name="moe",
    )(tokens, norm_gain.reshape(1, d_model), route, eg[0], eu[0], ed[0], sg, su, sd)


def solution(mesh):
    in_specs = (
        P(("ep", "tp"), None),
        P(),
        P(("ep", "tp"), None),
        P(("ep", "tp"), None),
        P("ep", "tp", None),
        P("ep", "tp", None),
        P("ep", "tp", None),
        P("tp", None),
        P("tp", None),
        P("tp", None),
    )
    out_specs = P(("ep", "tp"), None)
    return jax.shard_map(
        functools.partial(body, mesh.shape["ep"], mesh.shape["tp"]),
        mesh=mesh, in_specs=in_specs, out_specs=out_specs, check_vma=False,
    )
```

profile of v0, /device:TPU:0, one launch (start us, length us, event | category | flops | bytes accessed | tf_op | source)
XLA Modules:
  0.0 104.0 jit_solution(434288114910615915)
XLA Ops:
  0.0 0.0 copy-start
  0.0 0.7 copy-done
  0.7 0.0 copy-start.1
  0.7 0.7 copy-done.1
  1.4 0.7 copy.13.route_ref
  2.1 100.0 %moe.1 = bf16[128,2048]{1,0:T(8,128)(2,1)} custom-call(bf16[128,2048]{1,0:T(8,128)(2,1)} %tok_ref.1, f32[1,2048]{1,0:T(1,128)} %bitcast.7, f32[128,4]{1,0:T(8,128)} %copy.13.route_ref, bf16[128,2048]{1,0:T(8,128)(2,1)} %bitcast.4, bf16[128,2048]{1,0:T(8,128)(2,1)} %bitcast.5, bf16[128,2048]{1,0:T(8,128)(2,1)} %bitcast.6, bf16[128,2048]{1,0:T(8,128)(2,1)} %sg.1, ...), custom_call_target="tpu_custom_call" | custom-call | tf_op jit(solution)/shard_map/moe/pallas_call | solution.py:335
  102.1 1.9 %copy.15 = bf16[128,2048]{1,0:T(8,128)(2,1)} copy(bf16[128,2048]{1,0:T(8,128)(2,1)} %moe.1) | data formatting | bytes 1048576
  (2 shorter events, 0.0 us)
Async XLA Ops:
  0.0 0.7 copy-start
  0.7 0.7 copy-start.1
where the time goes:
time: 104 us
  Pallas kernels  100 us (96%)
  local copies, waits for them, and re-layouts  3.98 us (4%)
    pallas_call x1, Pallas kernels, body(): pl.pallas_call(functools.partial(kernel, ep, tp, xs, ys, cap), out_shape=...  100 us
    unnamed x5, local copies, waits for them, and re-layouts  3.24 us

commit v1 on v0

v1 whole, which is shorter than its diff:
```python
import functools
import math

import jax
import jax.numpy as jnp
from jax import lax
from jax.experimental import pallas as pl
from jax.experimental.pallas import tpu as pltpu
from jax.sharding import PartitionSpec as P

EPS = 1e-06
MESH = pl.DeviceIdType.MESH
NT = (((1,), (1,)), ((), ()))
F32 = jnp.float32
BF16 = jnp.bfloat16
CHUNKS = 8
SPIECES = 2
REACH = 2


def remote(src, dst, send, recv, where):
    return pltpu.make_async_remote_copy(
        src_ref=src, dst_ref=dst, send_sem=send, recv_sem=recv, device_id=where, device_id_type=MESH
    )


def runs_of(slots):
    out = []
    for s in slots:
        if out and out[-1][1] == s:
            out[-1][1] = s + 1
        else:
            out.append([s, s + 1])
    return out


def kernel(
    ep, tp, xs, ys, nsh,
    tok_ref, gain_ref, ids_ref, gw_ref, eg, eu, ed, sg, su, sd, out_ref,
    tokv, act, wsend, wrecv, wcol, wts, swts, hid, shid, acc, fin, ring,
    lt, lw, ls, s1, r1, s2, r2, s3, r3, st, rt, sw, rw, sc, rc,
):
    e = lax.axis_index("ep")
    t = lax.axis_index("tp")
    y, x = t // xs, t % xs
    z, core = e // 2, e % 2
    nz = ep // 2
    partner = e + 1 - 2 * core
    rows, d_model = tok_ref.shape
    own_rows = eg.shape[0]
    srows = swts.shape[3]
    piece = d_model // CHUNKS
    spiece = d_model // SPIECES
    half_rows = rows // 2
    z0 = (nz - nsh) // 2
    last = 2 + CHUNKS
    sdown = last + 2
    shares = (z >= z0) & (z < z0 + nsh)

    def at(dy, dx):
        return lax.rem(y + dy, ys) * xs + lax.rem(x + dx, xs)

    def slot(dy, dx):
        return (dy % ys) * xs + dx % xs

    row_off = [(0, i) for i in range(1, xs)]
    col_off = [(i, 0) for i in range(1, ys)]
    near_off = row_off + col_off
    diag_off = [(i, j) for i in range(1, ys) for j in range(1, xs)]
    near_slots = sorted([0] + [slot(*o) for o in near_off])
    diag_slots = sorted(slot(*o) for o in diag_off)

    mine = pl.ds(pl.multiple_of(((z - z0) * 2 + core) * srows, srows), srows)
    loads = [
        pltpu.make_async_copy(tok_ref, tokv, lt.at[0]),
        pltpu.make_async_copy(eg, wts.at[0, core, 0], lw.at[0]),
        pltpu.make_async_copy(eu, wts.at[1, core, 0], lw.at[1]),
        pltpu.make_async_copy(ed, wts.at[2, core, 0], lw.at[2]),
    ]
    for c in loads:
        c.start()
    sloads = [pltpu.make_async_copy(r.at[mine], swts.at[i, core, 0], ls.at[i]) for i, r in enumerate((sg, su, sd))]

    @pl.when(shares)
    def _():
        for c in sloads:
            c.start()

    barrier = pltpu.get_barrier_semaphore()
    for o in near_off:
        pl.semaphore_signal(barrier, inc=1, device_id={"tp": at(*o)}, device_id_type=MESH)
    for i in range(1, nz):
        pl.semaphore_signal(barrier, inc=1, device_id={"ep": lax.rem(e + 2 * i, ep)}, device_id_type=MESH)
    pl.semaphore_signal(barrier, inc=1, device_id={"ep": partner}, device_id_type=MESH)

    chosen = ids_ref.shape[0]
    sub = lax.broadcasted_iota(jnp.int32, (8, rows), 0)
    for p in range(nz):
        label = sub + 2 * p
        total = jnp.zeros((8, rows), F32)
        for k in range(chosen):
            total = total + jnp.where(ids_ref[k : k + 1, :] == label, gw_ref[k : k + 1, :], 0.0)
        wsend[p] = total
    loads[0].wait()
    tok = tokv[...].astype(F32)
    nrm = tok * lax.rsqrt(jnp.mean(tok * tok, axis=-1, keepdims=True) + EPS) * gain_ref[...]
    act[z] = nrm.astype(BF16)
    for c in loads[1:]:
        c.wait()

    @pl.when(shares)
    def _():
        for c in sloads:
            c.wait()

    pl.semaphore_wait(barrier, len(near_off) + nz)

    sends = []
    ssends = []

    def columns(a):
        if 2 <= a < last:
            return (a - 2) * piece, piece
        if a >= sdown:
            return (a - sdown) * spiece, spiece
        return 0, d_model

    def view(a, k, s, start, size):
        cols = pl.ds(start, size)
        if a < last:
            return wts.at[min(a, 2), k, s, :, cols]
        return swts.at[min(a - last, 2), k, s, :, cols]

    def block(a, k, s):
        return view(a, k, s, *columns(a))

    def part(a, s, h):
        start, size = columns(a)
        return view(a, core, s, start + h * (size // 2), size // 2)

    def keep(a, *parts):
        make = functools.partial(copy_of, a, *parts)
        (sends if a < last else ssends).append(make)
        make().start()

    def copy_of(a, kind, *where):
        if kind == "over":
            (s,) = where
            return remote(block(a, core, s), block(a, core, s), s3.at[a, s], r3.at[a, s], {"ep": partner})
        if kind == "first":
            j, (dy, dx) = where
            to = slot(-dy, -dx)
            return remote(block(a, core, 0), block(a, core, to), s1.at[a, j], r1.at[a, to], {"tp": at(dy, dx)})
        h, i, j, (oy, ox), (py, px) = where
        to = slot(oy - py, ox - px)
        return remote(part(a, slot(oy, ox), h), part(a, to, h), s2.at[a, h, i, j], r2.at[a, h, to], {"tp": at(py, px)})

    def over(a, s):
        keep(a, "over", s)

    def first(a):
        for j, o in enumerate(near_off):
            keep(a, "first", j, o)

    def first_done(a):
        for o in near_off:
            s = slot(*o)
            remote(block(a, core, s), block(a, core, s), s1.at[a, 0], r1.at[a, s], {"tp": t}).wait_recv()

    def second(a):
        for h, (owners, peers) in enumerate(((col_off, row_off), (row_off, col_off))):
            for i, o in enumerate(owners):
                for j, p in enumerate(peers):
                    keep(a, "second", h, i, j, o, p)

    def second_done(a):
        for s in diag_slots:
            for h in range(2):
                remote(part(a, s, h), part(a, s, h), s2.at[a, h, 0, 0], r2.at[a, h, s], {"tp": t}).wait_recv()

    def over_done(a, slots):
        for s in slots:
            b = block(a, 1 - core, s)
            remote(b, b, s3.at[a, s], r3.at[a, s], {"ep": partner}).wait_recv()

    def relay(a):
        first_done(a)
        second(a)
        for s in near_slots[1:]:
            over(a, s)

    def finish(a):
        second_done(a)
        for s in diag_slots:
            over(a, s)

    def hop(src, h, sign):
        ref = act.at[src, pl.ds(h * half_rows, half_rows), :]
        return remote(ref, ref, st.at[0 if sign > 0 else 1, src, h], rt.at[src, h], {"ep": e + 2 * sign})

    def travel(step, h, act_on):
        for sign in (1, -1):
            src = z - sign * step
            there = (src >= 0) if sign > 0 else (src < nz)
            on = (z + 1 < nz) if sign > 0 else (z > 0)
            act_on(src, h, sign, there, on)

    def pass_on(src, h, sign, there, on):
        @pl.when(there)
        def _():
            hop(src, h, sign).wait_recv()

            @pl.when(on)
            def _():
                hop(src, h, sign).start()

    first(0)
    for h in range(2):
        for sign in (1, -1):
            on = (z + 1 < nz) if sign > 0 else (z > 0)

            @pl.when(on)
            def _():
                hop(z, h, sign).start()

    over(0, 0)
    over(1, 0)
    first(1)
    for i in range(1, nz):
        p = lax.rem(z + i, nz)
        c = remote(wsend.at[p], wrecv.at[z], sw.at[i], rw.at[z], {"ep": 2 * p + core})
        c.start()
    wrecv[z] = wsend[z]
    for n in range(CHUNKS):
        over(2 + n, 0)

    for i in range(1, nz):
        p = lax.rem(z + i, nz)
        remote(wrecv.at[p], wrecv.at[p], sw.at[0], rw.at[p], {"ep": e}).wait_recv()

    def turn(p, carry):
        wcol[p] = wrecv[p].T
        return carry

    lax.fori_loop(0, nz, turn, 0)

    def ffn(p, planes, groups):
        m = planes * rows
        held = act[pl.ds(p, planes)].reshape(m, d_model)
        scale = wcol[pl.ds(p, planes)].reshape(m, 8)
        for k in range(2):
            for lo, hi in groups:
                width = (hi - lo) * own_rows
                gate = lax.dot_general(held, wts[0, k, lo:hi].reshape(width, d_model), NT, preferred_element_type=F32)
                up = lax.dot_general(held, wts[1, k, lo:hi].reshape(width, d_model), NT, preferred_element_type=F32)
                val = gate * (1.0 / (1.0 + jnp.exp(-gate))) * up * scale[:, k : k + 1]
                base = (k * tp + lo) * own_rows
                hid[pl.ds(p, planes), :, base : base + width] = val.astype(BF16).reshape(planes, rows, width)

    def ffn_loop(lo, hi, groups):
        def step(p, carry):
            ffn(p, 1, groups)
            return carry

        lax.fori_loop(lo, hi, step, 0)

    staged = own_rows % 128 == 0
    pack = math.gcd(nz, 4)

    for h in range(2):
        travel(1, h, pass_on)
    relay(0)
    for h in range(2):
        if nz > 2:
            travel(2, h, pass_on)
    relay(1)

    @pl.when(shares)
    def _():
        first(last)
        first(last + 1)

    first(2)
    first(3)
    over_done(0, near_slots)
    over_done(1, near_slots)
    low = jnp.maximum(z - REACH, 0)
    high = jnp.minimum(z + REACH + 1, nz)
    if staged:
        ffn_loop(low, high, runs_of(near_slots))
    if nz > 3:
        travel(3, 0, pass_on)
    finish(0)
    if nz > 3:
        travel(3, 1, pass_on)
    for step in range(4, nz):
        for h in range(2):
            travel(step, h, pass_on)
    if staged:
        ffn_loop(0, low, runs_of(near_slots))
        ffn_loop(high, nz, runs_of(near_slots))
    finish(1)

    @pl.when(shares)
    def _():
        relay(last)
        relay(last + 1)
        over(last, 0)
        over(last + 1, 0)
        for n in range(SPIECES):
            over(sdown + n, 0)
        first(sdown)

    relay(2)
    first(4)
    over_done(0, diag_slots)
    over_done(1, diag_slots)
    tail = diag_slots if staged else list(range(tp))

    def late(i, carry):
        ffn(i * pack, pack, runs_of(tail))
        return carry

    lax.fori_loop(0, nz // pack, late, 0)
    all_slots = near_slots + diag_slots

    @pl.when(shares)
    def _():
        finish(last)
        finish(last + 1)
        relay(sdown)
        for n in range(1, SPIECES):
            first(sdown + n)
        over_done(last, all_slots)
        over_done(last + 1, all_slots)
        sall = 2 * tp * srows

        def shared(i, carry):
            held = act[pl.ds(i * pack, pack)].reshape(pack * rows, d_model)
            gate = lax.dot_general(held, swts[0].reshape(sall, d_model), NT, preferred_element_type=F32)
            up = lax.dot_general(held, swts[1].reshape(sall, d_model), NT, preferred_element_type=F32)
            val = gate * (1.0 / (1.0 + jnp.exp(-gate))) * up
            shid[pl.ds(i * pack, pack)] = val.astype(BF16).reshape(pack, rows, sall)
            return carry

        lax.fori_loop(0, nz // pack, shared, 0)

    def link(n, d, sign, j):
        cols = pl.ds(n * piece, piece)
        to = nz if (sign < 0 and j == 1) else d
        return remote(ring.at[d, :, cols], ring.at[to, :, cols], sc.at[n, d], rc.at[n, to], {"ep": e + 2 * sign})

    def landed(n, s):
        ref = ring.at[s, :, pl.ds(n * piece, piece)]
        remote(ref, ref, sc.at[n, 0], rc.at[n, s], {"ep": e}).wait_recv()

    def each_link(run):
        for j in range(nz - 1, 0, -1):
            for sign in (1, -1):
                d = z + sign * j
                there = (d < nz) if sign > 0 else (d >= 0)
                fed = (z > 0) if sign > 0 else (z < nz - 1)

                @pl.when(there)
                def _():
                    run(d, sign, j, fed)

    for n in range(CHUNKS):
        lo, hi = n * piece, (n + 1) * piece
        finish(n + 2)
        over_done(n + 2, all_slots)
        if n % (CHUNKS // SPIECES) == 0:
            q = n // (CHUNKS // SPIECES)

            @pl.when(shares)
            def _():
                if q > 0:
                    relay(sdown + q)
                finish(sdown + q)
                over_done(sdown + q, all_slots)

        def down(i, carry):
            left = hid[pl.ds(i * pack, pack)].reshape(pack * rows, 2 * tp * own_rows)
            right = wts[2, :, :, :, lo:hi].reshape(2 * tp * own_rows, piece)
            o = jnp.dot(left, right, preferred_element_type=F32)
            acc[pl.ds(i * pack, pack)] = o.reshape(pack, rows, piece)

            @pl.when(shares)
            def _():
                more = jnp.dot(
                    shid[pl.ds(i * pack, pack)].reshape(pack * rows, 2 * tp * srows),
                    swts[2, :, :, :, lo:hi].reshape(2 * tp * srows, piece),
                    preferred_element_type=F32,
                )
                acc[pl.ds(i * pack, pack)] += more.reshape(pack, rows, piece)

            return carry

        lax.fori_loop(0, nz // pack, down, 0)
        fin[:, lo:hi] = acc[z]

        if n + 3 < last:
            relay(n + 3)
        if n + 5 < last:
            first(n + 5)

        def run(d, sign, j, fed):
            @pl.when(fed)
            def _():
                landed(n, d)
                ring[d, :, lo:hi] = (acc[d] + ring[d, :, lo:hi].astype(F32)).astype(BF16)

            @pl.when(jnp.logical_not(fed))
            def _():
                ring[d, :, lo:hi] = acc[d].astype(BF16)

            link(n, d, sign, j).start()

        each_link(run)

    for n in range(CHUNKS):
        lo, hi = n * piece, (n + 1) * piece

        @pl.when(z > 0)
        def _():
            landed(n, z)
            fin[:, lo:hi] += ring[z, :, lo:hi].astype(F32)

        @pl.when(z < nz - 1)
        def _():
            landed(n, nz)
            fin[:, lo:hi] += ring[nz, :, lo:hi].astype(F32)

        out_ref[:, lo:hi] = fin[:, lo:hi].astype(BF16)

    for i in range(1, nz):
        p = lax.rem(z + i, nz)
        remote(wsend.at[p], wrecv.at[z], sw.at[i], rw.at[z], {"ep": 2 * p + core}).wait_send()
    for make in sends:
        make().wait_send()

    @pl.when(shares)
    def _():
        for make in ssends:
            make().wait_send()

    for n in range(CHUNKS):
        each_link(lambda d, sign, j, fed: link(n, d, sign, j).wait_send())

    for h in range(2):
        for sign in (1, -1):
            on = (z + 1 < nz) if sign > 0 else (z > 0)

            @pl.when(on)
            def _():
                hop(z, h, sign).wait_send()

        for step in range(1, nz):

            def sent(src, h, sign, there, on):
                @pl.when(there & on)
                def _():
                    hop(src, h, sign).wait_send()

            travel(step, h, sent)


def body(ep, tp, tokens, norm_gain, expert_ids, gate_weights, eg, eu, ed, sg, su, sd):
    rows, d_model = tokens.shape
    side = math.isqrt(tp)
    xs = side if side * side == tp else tp
    ys = tp // xs
    nz = ep // 2
    own_rows = eg.shape[1]
    nsh = max(1, min(sg.shape[0] // 32, nz - 2))
    srows = sg.shape[0] // (2 * nsh)
    near = xs + ys - 2
    far = max(xs, ys)
    moves = 2 + CHUNKS + 2 + SPIECES
    dma = pltpu.SemaphoreType.DMA
    vm = pl.BlockSpec(memory_space=pltpu.VMEM)
    hbm = pl.BlockSpec(memory_space=pl.ANY)
    return pl.pallas_call(
        functools.partial(kernel, ep, tp, xs, ys, nsh),
        out_shape=jax.ShapeDtypeStruct((rows, d_model), BF16),
        in_specs=[hbm, vm, vm, vm] + [hbm] * 6,
        out_specs=vm,
        scratch_shapes=[
            pltpu.VMEM((rows, d_model), BF16),
            pltpu.VMEM((nz, rows, d_model), BF16),
            pltpu.VMEM((nz, 8, rows), F32),
            pltpu.VMEM((nz, 8, rows), F32),
            pltpu.VMEM((nz, rows, 8), F32),
            pltpu.VMEM((3, 2, tp, own_rows, d_model), BF16),
            pltpu.VMEM((3, 2, tp, srows, d_model), BF16),
            pltpu.VMEM((nz, rows, 2 * tp * own_rows), BF16),
            pltpu.VMEM((nz, rows, 2 * tp * srows), BF16),
            pltpu.VMEM((nz, rows, d_model // CHUNKS), F32),
            pltpu.VMEM((rows, d_model), F32),
            pltpu.VMEM((nz + 1, rows, d_model), BF16),
            dma((1,)),
            dma((3,)),
            dma((3,)),
            dma((moves, near)),
            dma((moves, tp)),
            dma((moves, 2, far, far)),
            dma((moves, 2, tp)),
            dma((moves, tp)),
            dma((moves, tp)),
            dma((2, nz, 2)),
            dma((nz, 2)),
            dma((nz,)),
            dma((nz,)),
            dma((CHUNKS, nz)),
            dma((CHUNKS, nz + 1)),
        ],
        compiler_params=pltpu.CompilerParams(
            collective_id=0, has_side_effects=True, vmem_limit_bytes=62 * 1024 * 1024
        ),
        name="moe",
    )(tokens, norm_gain.reshape(1, d_model), expert_ids.T, gate_weights.T, eg[0], eu[0], ed[0], sg, su, sd)


def solution(mesh):
    in_specs = (
        P(("ep", "tp"), None),
        P(),
        P(("ep", "tp"), None),
        P(("ep", "tp"), None),
        P("ep", "tp", None),
        P("ep", "tp", None),
        P("ep", "tp", None),
        P("tp", None),
        P("tp", None),
        P("tp", None),
    )
    out_specs = P(("ep", "tp"), None)
    return jax.shard_map(
        functools.partial(body, mesh.shape["ep"], mesh.shape["tp"]),
        mesh=mesh, in_specs=in_specs, out_specs=out_specs, check_vma=False,
    )
```

time: 104 us -> 114 us (1.096)
  Pallas kernels: 100 us -> 112 us
  local copies, waits for them, and re-layouts: 3.98 us -> 1.88 us
    pallas_call x1, Pallas kernels: 100 us -> 112 us  [body(): pl.pallas_call(functools.partial(kernel, ep, tp, xs, ys, nsh), out_shape=...]
    unnamed x5 -> x1, local copies, waits for them, and re-layouts: 3.24 us -> 1.88 us
where the time goes in v1:
time: 114 us
  Pallas kernels  112 us (98%)
  local copies, waits for them, and re-layouts  1.88 us (2%)
    pallas_call x1, Pallas kernels, body(): pl.pallas_call(functools.partial(kernel, ep, tp, xs, ys, nsh), out_shape=...  112 us

profile of v1, /device:TPU:0, one launch (start us, length us, event | category | flops | bytes accessed | tf_op | source)
XLA Modules:
  0.0 114.0 jit_solution(17590096800442397587)
XLA Ops:
  0.0 112.1 %moe.1 = bf16[128,2048]{1,0:T(8,128)(2,1)} custom-call(bf16[128,2048]{1,0:T(8,128)(2,1)} %tok_ref.1, f32[1,2048]{1,0:T(1,128)} %bitcast.9, s32[2,128]{1,0:T(2,128)} %bitcast.10, f32[2,128]{1,0:T(2,128)} %bitcast.11, bf16[128,2048]{1,0:T(8,128)(2,1)} %bitcast.6, bf16[128,2048]{1,0:T(8,128)(2,1)} %bitcast.7, bf16[128,2048]{1,0:T(8,128)(2,1)} %bitcast.8, ...), custom_call_target="tpu_custom_call" | custom-call | tf_op jit(solution)/shard_map/moe/pallas_call | solution.py:483
  112.1 1.9 %copy.12 = bf16[128,2048]{1,0:T(8,128)(2,1)} copy(bf16[128,2048]{1,0:T(8,128)(2,1)} %moe.1) | data formatting | bytes 1048576

commit v2 on v1

v2 whole, which is shorter than its diff:
```python
import functools
import math

import jax
import jax.numpy as jnp
from jax import lax
from jax.experimental import pallas as pl
from jax.experimental.pallas import tpu as pltpu
from jax.sharding import PartitionSpec as P

EPS = 1e-06
MESH = pl.DeviceIdType.MESH
NT = (((1,), (1,)), ((), ()))
F32 = jnp.float32
BF16 = jnp.bfloat16
CHUNKS = 8
SPIECES = 2
REACH = 2
PIECES = ((0, 1), (1, 1), (2, 2), (4, 2), (6, 2))


def remote(src, dst, send, recv, where):
    return pltpu.make_async_remote_copy(
        src_ref=src, dst_ref=dst, send_sem=send, recv_sem=recv, device_id=where, device_id_type=MESH
    )


def runs_of(slots):
    out = []
    for s in slots:
        if out and out[-1][1] == s:
            out[-1][1] = s + 1
        else:
            out.append([s, s + 1])
    return out


def kernel(
    ep, tp, xs, ys, nsh,
    tok_ref, gain_ref, ids_ref, gw_ref, eg, eu, ed, sg, su, sd, out_ref,
    tokv, act, wtab, wcol, wts, swts, gbuf, hid, shid, acc, fin, ring,
    ld, sx, r1, r2, r3, r4, st, rt, sw, rw, sc, rc,
):
    e = lax.axis_index("ep")
    t = lax.axis_index("tp")
    y, x = t // xs, t % xs
    z, core = e // 2, e % 2
    nz = ep // 2
    partner = e + 1 - 2 * core
    rows, d_model = tok_ref.shape
    own_rows = eg.shape[0]
    srows = swts.shape[3]
    piece = d_model // CHUNKS
    spiece = d_model // SPIECES
    half_rows = rows // 2
    z0 = (nz - nsh) // 2
    parts = len(PIECES)
    last = 2 + parts
    sdown = last + 1
    shares = (z >= z0) & (z < z0 + nsh)

    def at(dy, dx):
        return lax.rem(y + dy, ys) * xs + lax.rem(x + dx, xs)

    def slot(dy, dx):
        return (dy % ys) * xs + dx % xs

    row_off = [(0, i) for i in range(1, xs)]
    col_off = [(i, 0) for i in range(1, ys)]
    near_off = row_off + col_off
    near_slots = sorted([0] + [slot(*o) for o in near_off])
    diag_slots = [s for s in range(tp) if s not in near_slots]
    near, ndiag = len(near_off), len(diag_slots)

    mine = pl.ds(pl.multiple_of(((z - z0) * 2 + core) * srows, srows), srows)
    loads = [
        pltpu.make_async_copy(tok_ref, tokv, ld.at[0]),
        pltpu.make_async_copy(eg, wts.at[0, 0, core], ld.at[1]),
        pltpu.make_async_copy(eu, wts.at[1, 0, core], ld.at[2]),
        pltpu.make_async_copy(ed, wts.at[2, 0, core], ld.at[3]),
    ]
    for c in loads:
        c.start()
    sloads = [pltpu.make_async_copy(r.at[mine], swts.at[i, 0, core], ld.at[4 + i]) for i, r in enumerate((sg, su, sd))]

    @pl.when(shares)
    def _():
        for c in sloads:
            c.start()

    barrier = pltpu.get_barrier_semaphore()
    for o in near_off:
        pl.semaphore_signal(barrier, inc=1, device_id={"tp": at(*o)}, device_id_type=MESH)
    pl.semaphore_signal(barrier, inc=1, device_id={"ep": partner}, device_id_type=MESH)
    for sign in (1, -1):
        on = (z + 1 < nz) if sign > 0 else (z > 0)

        @pl.when(on)
        def _():
            pl.semaphore_signal(barrier, inc=1, device_id={"ep": e + 2 * sign}, device_id_type=MESH)

    chosen = ids_ref.shape[0]
    label = lax.broadcasted_iota(jnp.int32, wtab.shape[1:], 0)
    total = jnp.zeros(wtab.shape[1:], F32)
    for k in range(chosen):
        total = total + jnp.where(ids_ref[k : k + 1, :] == label, gw_ref[k : k + 1, :], 0.0)
    wtab[z] = total
    loads[0].wait()
    tok = tokv[...].astype(F32)
    nrm = tok * lax.rsqrt(jnp.mean(tok * tok, axis=-1, keepdims=True) + EPS) * gain_ref[...]
    act[z] = nrm.astype(BF16)
    for c in loads[1:]:
        c.wait()

    @pl.when(shares)
    def _():
        for c in sloads:
            c.wait()

    pl.semaphore_wait(barrier, near + 1 + (z > 0).astype(jnp.int32) + (z < nz - 1).astype(jnp.int32))

    def columns(a):
        if 2 <= a < last:
            lo, count = PIECES[a - 2]
            return lo * piece, count * piece
        if a >= sdown:
            return (a - sdown) * spiece, spiece
        return 0, d_model

    def view(a, s, k, start, size):
        cols = pl.ds(start, size)
        if a < last:
            return wts.at[min(a, 2), s, k, :, cols]
        if a == last:
            return swts.at[pl.ds(0, 2), s, k, :, cols]
        return swts.at[2, s, k, :, cols]

    def block(a, s, k):
        return view(a, s, k, *columns(a))

    def part(a, s, h):
        start, size = columns(a)
        return view(a, s, core, start + h * (size // 2), size // 2)

    def first(a):
        for dy, dx in near_off:
            to = slot(-dy, -dx)
            remote(block(a, 0, core), block(a, to, core), sx.at[int(a >= last), 0], r1.at[a], {"tp": at(dy, dx)}).start()

    def second(a):
        for h, (owners, peers) in enumerate(((col_off, row_off), (row_off, col_off))):
            for oy, ox in owners:
                for py, px in peers:
                    to = slot(oy - py, ox - px)
                    remote(part(a, slot(oy, ox), h), part(a, to, h), sx.at[int(a >= last), 1], r2.at[a], {"tp": at(py, px)}).start()

    def over(a, slots, sem):
        for s in slots:
            b = block(a, s, core)
            remote(b, b, sx.at[int(a >= last), 2], sem, {"ep": partner}).start()

    def arrive(ref, sem):
        remote(ref, ref, sx.at[0, 0], sem, {"ep": partner}).wait_recv()

    def relay(a):
        arrive(block(a, pl.ds(0, near), core), r1.at[a])
        second(a)
        over(a, near_slots[1:], r3.at[a, 0])

    def finish(a):
        arrive(block(a, pl.ds(0, ndiag), core), r2.at[a])
        over(a, diag_slots, r3.at[a, 1])

    def near_over(a):
        arrive(block(a, pl.ds(0, near), 1 - core), r3.at[a, 0])

    def diag_over(a):
        arrive(block(a, pl.ds(0, ndiag), 1 - core), r3.at[a, 1])

    def token_copy(src, h, sign, sem):
        ref = act.at[src, pl.ds(h * half_rows, half_rows), :]
        return remote(ref, ref, st.at[sem], rt.at[src, h], {"ep": e + 2 * sign})

    def table_copy(src, sign, sem):
        return remote(wtab.at[src], wtab.at[src], sw.at[sem], rw.at[src], {"ep": e + 2 * sign})

    def travel(step, h):
        for sign in (1, -1):
            src = z - sign * step
            there = (src >= 0) if sign > 0 else (src < nz)
            on = (z + 1 < nz) if sign > 0 else (z > 0)

            @pl.when(there)
            def _():
                if h == 0:
                    table_copy(src, sign, src).wait_recv()
                    wcol[src] = wtab[src].T

                    @pl.when(on)
                    def _():
                        table_copy(src, sign, src).start()

                token_copy(src, h, sign, src).wait_recv()

                @pl.when(on)
                def _():
                    token_copy(src, h, sign, src).start()

    def own_tokens(run):
        for sign in (1, -1):
            on = (z + 1 < nz) if sign > 0 else (z > 0)
            sem = z if sign > 0 else nz

            @pl.when(on)
            def _():
                run(sign, sem)

    own_tokens(lambda sign, sem: table_copy(z, sign, sem).start())
    first(0)
    for h in range(2):
        own_tokens(lambda sign, sem: token_copy(z, h, sign, sem).start())
    over(0, [0], r4.at[0])
    over(1, [0], r4.at[0])
    first(1)
    first(2)

    @pl.when(shares)
    def _():
        first(last)
        over(last, [0], r4.at[2])
        own = swts.at[2, 0, core]
        remote(own, own, sx.at[1, 2], r4.at[3], {"ep": partner}).start()

    own = wts.at[2, 0, core]
    remote(own, own, sx.at[0, 2], r4.at[1], {"ep": partner}).start()
    wcol[z] = wtab[z].T

    lanes = lax.broadcasted_iota(jnp.int32, (1, wcol.shape[2]), 1)

    def weighted(gate, up, p, planes):
        m, width = gate.shape
        col = wcol[pl.ds(p, planes)].reshape(m, wcol.shape[2])
        pair = [jnp.sum(jnp.where(lanes == 2 * z + k, col, 0.0), axis=1, keepdims=True) for k in range(2)]
        which = lax.broadcasted_iota(jnp.int32, (1, width), 1) // own_rows % 2
        scale = jnp.where(which == 0, pair[0], pair[1])
        val = gate * (1.0 / (1.0 + jnp.exp(-gate))) * up * scale
        return val.astype(BF16).reshape(planes, rows, width)

    def project(a, p, planes, lo, hi):
        held = act[pl.ds(p, planes)].reshape(planes * rows, d_model)
        weight = wts[a, lo:hi].reshape((hi - lo) * 2 * own_rows, d_model)
        return lax.dot_general(held, weight, NT, preferred_element_type=F32)

    def ffn(p, planes, groups):
        for lo, hi in groups:
            val = weighted(project(0, p, planes, lo, hi), project(1, p, planes, lo, hi), p, planes)
            hid[pl.ds(p, planes), :, lo * 2 * own_rows : hi * 2 * own_rows] = val

    def ffn_loop(lo, hi, groups):
        def step(p, carry):
            ffn(p, 1, groups)
            return carry

        lax.fori_loop(lo, hi, step, 0)

    staged = own_rows % 128 == 0 and len(runs_of(near_slots)) == 1
    pack = math.gcd(nz, 4)
    low = jnp.maximum(z - REACH, 0)
    high = jnp.minimum(z + REACH + 1, nz)
    dlo, dhi = min(diag_slots), max(diag_slots) + 1

    for h in range(2):
        travel(1, h)
    relay(0)
    if nz > 2:
        for h in range(2):
            travel(2, h)
    relay(1)
    relay(2)

    @pl.when(shares)
    def _():
        relay(last)
        first(sdown)

    first(3)
    first(4)
    arrive(wts.at[pl.ds(0, 2), 0, 1 - core], r4.at[0])
    near_over(0)
    near_over(1)
    if staged:
        ffn_loop(low, high, runs_of(near_slots))
    if nz > 3:
        travel(3, 0)
    finish(0)
    finish(1)
    finish(2)
    if nz > 3:
        travel(3, 1)
    for step in range(4, nz):
        for h in range(2):
            travel(step, h)
    diag_over(0)

    def early(i, carry):
        gbuf[pl.ds(i * pack, pack)] = project(0, i * pack, pack, dlo, dhi).reshape(pack, rows, gbuf.shape[2])
        return carry

    if staged:
        ffn_loop(0, low, runs_of(near_slots))
        ffn_loop(high, nz, runs_of(near_slots))
        lax.fori_loop(0, nz // pack, early, 0)
    diag_over(1)

    def late(i, carry):
        p = i * pack
        if staged:
            gate = gbuf[pl.ds(p, pack)].reshape(pack * rows, gbuf.shape[2])
            val = weighted(gate, project(1, p, pack, dlo, dhi), p, pack)
            hid[pl.ds(p, pack), :, dlo * 2 * own_rows : dhi * 2 * own_rows] = val
        else:
            ffn(p, pack, [(0, tp)])
        return carry

    lax.fori_loop(0, nz // pack, late, 0)
    arrive(wts.at[2, 0, 1 - core], r4.at[1])
    near_over(2)
    relay(3)
    first(5)

    @pl.when(shares)
    def _():
        finish(last)
        relay(sdown)
        for n in range(1, SPIECES):
            first(sdown + n)
        arrive(swts.at[pl.ds(0, 2), 0, 1 - core], r4.at[2])
        arrive(swts.at[2, 0, 1 - core], r4.at[3])
        near_over(last)
        diag_over(last)
        sall = 2 * tp * srows

        def shared(i, carry):
            held = act[pl.ds(i * pack, pack)].reshape(pack * rows, d_model)
            gate = lax.dot_general(held, swts[0].reshape(sall, d_model), NT, preferred_element_type=F32)
            up = lax.dot_general(held, swts[1].reshape(sall, d_model), NT, preferred_element_type=F32)
            val = gate * (1.0 / (1.0 + jnp.exp(-gate))) * up
            shid[pl.ds(i * pack, pack)] = val.astype(BF16).reshape(pack, rows, sall)
            return carry

        lax.fori_loop(0, nz // pack, shared, 0)
        finish(sdown)
        near_over(sdown)

    def link(n, d, sign, j):
        cols = pl.ds(n * piece, piece)
        to = nz if (sign < 0 and j == 1) else d
        return remote(ring.at[d, :, cols], ring.at[to, :, cols], sc.at[d], rc.at[n, to], {"ep": e + 2 * sign})

    def landed(n, s):
        arrive(ring.at[s, :, pl.ds(n * piece, piece)], rc.at[n, s])

    def each_link(run):
        for j in range(nz - 1, 0, -1):
            for sign in (1, -1):
                d = z + sign * j
                there = (d < nz) if sign > 0 else (d >= 0)
                depth = z if sign > 0 else nz - 1 - z
                run(d, sign, j, there, depth)

    def send_on(n, lagged):
        lo, hi = n * piece, (n + 1) * piece

        def run(d, sign, j, there, depth):
            @pl.when(there & ((depth >= 2) if lagged else (depth < 2)))
            def _():
                mine_now = acc[n % 2, d]

                @pl.when(depth > 0)
                def _():
                    landed(n, d)
                    ring[d, :, lo:hi] = (mine_now + ring[d, :, lo:hi].astype(F32)).astype(BF16)

                @pl.when(depth == 0)
                def _():
                    ring[d, :, lo:hi] = mine_now.astype(BF16)

                link(n, d, sign, j).start()

        each_link(run)

    starts = {lo: p for p, (lo, count) in enumerate(PIECES)}
    for n in range(CHUNKS):
        lo, hi = n * piece, (n + 1) * piece
        if n in starts:
            p = starts[n]
            if p + 1 < parts:
                finish(2 + p + 1)
            if p + 2 < parts:
                relay(2 + p + 2)
            if p + 4 < parts:
                first(2 + p + 4)
            if p > 0:
                near_over(2 + p)
            diag_over(2 + p)
        q, rest = divmod(n, CHUNKS // SPIECES)
        if rest == 0:

            @pl.when(shares)
            def _():
                if q + 1 < SPIECES:
                    relay(sdown + q + 1)
                if q > 0:
                    finish(sdown + q)
                    near_over(sdown + q)
                diag_over(sdown + q)

        def down(i, carry):
            left = hid[pl.ds(i * pack, pack)].reshape(pack * rows, 2 * tp * own_rows)
            right = wts[2, :, :, :, lo:hi].reshape(2 * tp * own_rows, piece)
            o = jnp.dot(left, right, preferred_element_type=F32)
            acc[n % 2, pl.ds(i * pack, pack)] = o.reshape(pack, rows, piece)

            @pl.when(shares)
            def _():
                more = jnp.dot(
                    shid[pl.ds(i * pack, pack)].reshape(pack * rows, 2 * tp * srows),
                    swts[2, :, :, :, lo:hi].reshape(2 * tp * srows, piece),
                    preferred_element_type=F32,
                )
                acc[n % 2, pl.ds(i * pack, pack)] += more.reshape(pack, rows, piece)

            return carry

        lax.fori_loop(0, nz // pack, down, 0)
        fin[:, lo:hi] = acc[n % 2, z]
        send_on(n, False)
        if n > 0:
            send_on(n - 1, True)
    send_on(CHUNKS - 1, True)

    for n in range(CHUNKS):
        lo, hi = n * piece, (n + 1) * piece

        @pl.when(z > 0)
        def _():
            landed(n, z)
            fin[:, lo:hi] += ring[z, :, lo:hi].astype(F32)

        @pl.when(z < nz - 1)
        def _():
            landed(n, nz)
            fin[:, lo:hi] += ring[nz, :, lo:hi].astype(F32)

        out_ref[:, lo:hi] = fin[:, lo:hi].astype(BF16)

    def left(ref, sem):
        remote(ref, ref, sem, r1.at[0], {"ep": partner}).wait_send()

    for j, count in enumerate((near, ndiag, tp)):
        left(wts.at[:, pl.ds(0, count), core], sx.at[0, j])

        @pl.when(shares)
        def _():
            left(swts.at[:, pl.ds(0, count), core], sx.at[1, j])

    def sent(d, sign, j, there, depth):
        @pl.when(there)
        def _():
            left(ring.at[d], sc.at[d])

    each_link(sent)

    def own_sent(sign, sem):
        left(act.at[z], st.at[sem])
        left(wtab.at[z], sw.at[sem])

    own_tokens(own_sent)
    for step in range(1, nz):
        for sign in (1, -1):
            src = z - sign * step
            there = (src >= 0) if sign > 0 else (src < nz)
            on = (z + 1 < nz) if sign > 0 else (z > 0)

            @pl.when(there & on)
            def _():
                left(act.at[src], st.at[src])
                left(wtab.at[src], sw.at[src])


def body(ep, tp, tokens, norm_gain, expert_ids, gate_weights, eg, eu, ed, sg, su, sd):
    rows, d_model = tokens.shape
    side = math.isqrt(tp)
    xs = side if side * side == tp else tp
    ys = tp // xs
    nz = ep // 2
    own_rows = eg.shape[1]
    nsh = max(1, min(sg.shape[0] // 32, nz - 2))
    srows = sg.shape[0] // (2 * nsh)
    moves = 2 + len(PIECES) + 1 + SPIECES
    dma = pltpu.SemaphoreType.DMA
    vm = pl.BlockSpec(memory_space=pltpu.VMEM)
    hbm = pl.BlockSpec(memory_space=pl.ANY)
    return pl.pallas_call(
        functools.partial(kernel, ep, tp, xs, ys, nsh),
        out_shape=jax.ShapeDtypeStruct((rows, d_model), BF16),
        in_specs=[hbm, vm, vm, vm] + [hbm] * 6,
        out_specs=vm,
        scratch_shapes=[
            pltpu.VMEM((rows, d_model), BF16),
            pltpu.VMEM((nz, rows, d_model), BF16),
            pltpu.VMEM((nz, max(8, ep), rows), F32),
            pltpu.VMEM((nz, rows, max(8, ep)), F32),
            pltpu.VMEM((3, tp, 2, own_rows, d_model), BF16),
            pltpu.VMEM((3, tp, 2, srows, d_model), BF16),
            pltpu.VMEM((nz, rows, 2 * own_rows * (xs - 1) * (ys - 1)) if own_rows % 128 == 0 else (1, 8, 128), F32),
            pltpu.VMEM((nz, rows, 2 * tp * own_rows), BF16),
            pltpu.VMEM((nz, rows, 2 * tp * srows), BF16),
            pltpu.VMEM((2, nz, rows, d_model // CHUNKS), F32),
            pltpu.VMEM((rows, d_model), F32),
            pltpu.VMEM((nz + 1, rows, d_model), BF16),
            dma((7,)),
            dma((2, 3)),
            dma((moves,)),
            dma((moves,)),
            dma((moves, 2)),
            dma((4,)),
            dma((nz + 1,)),
            dma((nz, 2)),
            dma((nz + 1,)),
            dma((nz,)),
            dma((nz,)),
            dma((CHUNKS, nz + 1)),
        ],
        compiler_params=pltpu.CompilerParams(
            collective_id=0, has_side_effects=True, vmem_limit_bytes=62 * 1024 * 1024
        ),
        name="moe",
    )(tokens, norm_gain.reshape(1, d_model), expert_ids.T, gate_weights.T, eg[0], eu[0], ed[0], sg, su, sd)


def solution(mesh):
    in_specs = (
        P(("ep", "tp"), None),
        P(),
        P(("ep", "tp"), None),
        P(("ep", "tp"), None),
        P("ep", "tp", None),
        P("ep", "tp", None),
        P("ep", "tp", None),
        P("tp", None),
        P("tp", None),
        P("tp", None),
    )
    out_specs = P(("ep", "tp"), None)
    return jax.shard_map(
        functools.partial(body, mesh.shape["ep"], mesh.shape["tp"]),
        mesh=mesh, in_specs=in_specs, out_specs=out_specs, check_vma=False,
    )
```

time: 114 us -> 96.6 us (0.85)
  Pallas kernels: 112 us -> 94.5 us
    pallas_call x1, Pallas kernels: 112 us -> 94.5 us  [body(): pl.pallas_call(functools.partial(kernel, ep, tp, xs, ys, nsh), out_shape=...]
where the time goes in v2:
time: 96.6 us; the launch traced here: 96.4 us
  Pallas kernels  94.5 us (98%)
  local copies, waits for them, and re-layouts  1.88 us (2%)
    pallas_call x1, Pallas kernels, body(): pl.pallas_call(functools.partial(kernel, ep, tp, xs, ys, nsh), out_shape=...  94.5 us

profile of v2, /device:TPU:0, one launch (start us, length us, event | category | flops | bytes accessed | tf_op | source)
XLA Modules:
  0.0 96.4 jit_solution(11017408174882749596)
XLA Ops:
  0.0 94.5 %moe.1 = bf16[128,2048]{1,0:T(8,128)(2,1)} custom-call(bf16[128,2048]{1,0:T(8,128)(2,1)} %tok_ref.1, f32[1,2048]{1,0:T(1,128)} %bitcast.9, s32[2,128]{1,0:T(2,128)} %bitcast.10, f32[2,128]{1,0:T(2,128)} %bitcast.11, bf16[128,2048]{1,0:T(8,128)(2,1)} %bitcast.6, bf16[128,2048]{1,0:T(8,128)(2,1)} %bitcast.7, bf16[128,2048]{1,0:T(8,128)(2,1)} %bitcast.8, ...), custom_call_target="tpu_custom_call" | custom-call | tf_op jit(solution)/shard_map/moe/pallas_call | solution.py:504
  94.5 1.9 %copy.12 = bf16[128,2048]{1,0:T(8,128)(2,1)} copy(bf16[128,2048]{1,0:T(8,128)(2,1)} %moe.1) | data formatting | bytes 1048576

commit v3 on v2

--- a/solution.py
+++ b/solution.py
@@ -16,7 +16,8 @@
 CHUNKS = 8
 SPIECES = 2
 REACH = 2
-PIECES = ((0, 1), (1, 1), (2, 2), (4, 2), (6, 2))
+HOLD = (2, 1)
+PIECES = tuple((n, 1) for n in range(CHUNKS))
 
 
 def remote(src, dst, send, recv, where):
@@ -105,17 +106,6 @@
     for k in range(chosen):
         total = total + jnp.where(ids_ref[k : k + 1, :] == label, gw_ref[k : k + 1, :], 0.0)
     wtab[z] = total
-    loads[0].wait()
-    tok = tokv[...].astype(F32)
-    nrm = tok * lax.rsqrt(jnp.mean(tok * tok, axis=-1, keepdims=True) + EPS) * gain_ref[...]
-    act[z] = nrm.astype(BF16)
-    for c in loads[1:]:
-        c.wait()
-
-    @pl.when(shares)
-    def _():
-        for c in sloads:
-            c.wait()
 
     pl.semaphore_wait(barrier, near + 1 + (z > 0).astype(jnp.int32) + (z < nz - 1).astype(jnp.int32))
 
@@ -142,10 +132,10 @@
         start, size = columns(a)
         return view(a, s, core, start + h * (size // 2), size // 2)
 
-    def first(a):
+    def first(a, source=None):
         for dy, dx in near_off:
             to = slot(-dy, -dx)
-            remote(block(a, 0, core), block(a, to, core), sx.at[int(a >= last), 0], r1.at[a], {"tp": at(dy, dx)}).start()
+            remote(block(a, 0, core) if source is None else source, block(a, to, core), sx.at[int(a >= last), 0], r1.at[a], {"tp": at(dy, dx)}).start()
 
     def second(a):
         for h, (owners, peers) in enumerate(((col_off, row_off), (row_off, col_off))):
@@ -215,8 +205,14 @@
             def _():
                 run(sign, sem)
 
+    first(0, eg)
+    loads[0].wait()
+    tok = tokv[...].astype(F32)
+    nrm = tok * lax.rsqrt(jnp.mean(tok * tok, axis=-1, keepdims=True) + EPS) * gain_ref[...]
+    act[z] = nrm.astype(BF16)
     own_tokens(lambda sign, sem: table_copy(z, sign, sem).start())
-    first(0)
+    for c in loads[1:]:
+        c.wait()
     for h in range(2):
         own_tokens(lambda sign, sem: token_copy(z, h, sign, sem).start())
     over(0, [0], r4.at[0])
@@ -226,7 +222,11 @@
 
     @pl.when(shares)
     def _():
+        for c in sloads:
+            c.wait()
         first(last)
+        first(sdown)
+        first(3)
         over(last, [0], r4.at[2])
         own = swts.at[2, 0, core]
         remote(own, own, sx.at[1, 2], r4.at[3], {"ep": partner}).start()
@@ -256,13 +256,6 @@
             val = weighted(project(0, p, planes, lo, hi), project(1, p, planes, lo, hi), p, planes)
             hid[pl.ds(p, planes), :, lo * 2 * own_rows : hi * 2 * own_rows] = val
 
-    def ffn_loop(lo, hi, groups):
-        def step(p, carry):
-            ffn(p, 1, groups)
-            return carry
-
-        lax.fori_loop(lo, hi, step, 0)
-
     staged = own_rows % 128 == 0 and len(runs_of(near_slots)) == 1
     pack = math.gcd(nz, 4)
     low = jnp.maximum(z - REACH, 0)
@@ -273,26 +266,62 @@
         travel(1, h)
     relay(0)
     if nz > 2:
-        for h in range(2):
-            travel(2, h)
+        travel(2, 0)
+    arrive(wts.at[pl.ds(0, 2), 0, 1 - core], r4.at[0])
+    near_over(0)
+    if nz > 2:
+        travel(2, 1)
     relay(1)
     relay(2)
+
+    @pl.when(jnp.logical_not(shares))
+    def _():
+        first(3)
+        first(4)
+
+    near_over(1)
+    groups = runs_of(near_slots)
+    pairs = (low + 1) // 2, high // 2
+    singles = (low, low + low % 2), (high - high % 2, high)
+    beyond = (0, low), (high, nz)
+
+    def early(p, width):
+        gbuf[pl.ds(p, width)] = project(0, p, width, dlo, dhi).reshape(width, rows, gbuf.shape[2])
+
+    def planes_loop(span, width, run):
+        def step(p, carry):
+            run(p * width, width)
+            return carry
+
+        lax.fori_loop(*span, step, 0)
+
+    def near_ffn(p, width):
+        ffn(p, width, groups)
+
+    if staged:
+        planes_loop(pairs, 2, near_ffn)
 
     @pl.when(shares)
     def _():
         relay(last)
-        first(sdown)
-
-    first(3)
-    first(4)
-    arrive(wts.at[pl.ds(0, 2), 0, 1 - core], r4.at[0])
-    near_over(0)
-    near_over(1)
+        relay(sdown)
+        relay(3)
+        first(4)
+        first(5)
+        for n in range(1, SPIECES):
+            first(sdown + n)
+
+    finish(0)
     if staged:
-        ffn_loop(low, high, runs_of(near_slots))
+        for span in singles:
+            planes_loop(span, 1, near_ffn)
     if nz > 3:
         travel(3, 0)
-    finish(0)
+    diag_over(0)
+    if staged:
+        planes_loop(pairs, 2, early)
+        for span in singles:
+            planes_loop(span, 1, early)
     finish(1)
     finish(2)
     if nz > 3:
@@ -300,16 +329,18 @@
     for step in range(4, nz):
         for h in range(2):
             travel(step, h)
-    diag_over(0)
-
-    def early(i, carry):
-        gbuf[pl.ds(i * pack, pack)] = project(0, i * pack, pack, dlo, dhi).reshape(pack, rows, gbuf.shape[2])
-        return carry
-
     if staged:
-        ffn_loop(0, low, runs_of(near_slots))
-        ffn_loop(high, nz, runs_of(near_slots))
-        lax.fori_loop(0, nz // pack, early, 0)
+        for span in beyond:
+            planes_loop(span, 1, near_ffn)
+
+    @pl.when(jnp.logical_not(shares))
+    def _():
+        relay(3)
+        first(5)
+
+    if staged:
+        for span in beyond:
+            planes_loop(span, 1, early)
     diag_over(1)
 
     def late(i, carry):
@@ -325,18 +356,14 @@
     lax.fori_loop(0, nz // pack, late, 0)
     arrive(wts.at[2, 0, 1 - core], r4.at[1])
     near_over(2)
-    relay(3)
-    first(5)
 
     @pl.when(shares)
     def _():
-        finish(last)
-        relay(sdown)
-        for n in range(1, SPIECES):
-            first(sdown + n)
         arrive(swts.at[pl.ds(0, 2), 0, 1 - core], r4.at[2])
         arrive(swts.at[2, 0, 1 - core], r4.at[3])
         near_over(last)
+        finish(last)
+        finish(sdown)
         diag_over(last)
         sall = 2 * tp * srows
 
@@ -349,8 +376,6 @@
             return carry
 
         lax.fori_loop(0, nz // pack, shared, 0)
-        finish(sdown)
-        near_over(sdown)
 
     def link(n, d, sign, j):
         cols = pl.ds(n * piece, piece)
@@ -385,7 +410,21 @@
                 def _():
                     ring[d, :, lo:hi] = mine_now.astype(BF16)
 
-                link(n, d, sign, j).start()
+                if lagged or j > 1:
+                    link(n, d, sign, j).start()
+
+        each_link(run)
+
+    def send_late(n, wanted):
+        if not 0 <= n < CHUNKS:
+            return
+
+        def run(d, sign, j, there, depth):
+            if j == 1:
+
+                @pl.when(there & (depth == wanted))
+                def _():
+                    link(n, d, sign, j).start()
 
         each_link(run)
 
@@ -393,26 +432,13 @@
     for n in range(CHUNKS):
         lo, hi = n * piece, (n + 1) * piece
         if n in starts:
-            p = starts[n]
-            if p + 1 < parts:
-                finish(2 + p + 1)
-            if p + 2 < parts:
-                relay(2 + p + 2)
-            if p + 4 < parts:
-                first(2 + p + 4)
-            if p > 0:
-                near_over(2 + p)
-            diag_over(2 + p)
+            diag_over(2 + starts[n])
         q, rest = divmod(n, CHUNKS // SPIECES)
         if rest == 0:
 
             @pl.when(shares)
             def _():
-                if q + 1 < SPIECES:
-                    relay(sdown + q + 1)
-                if q > 0:
-                    finish(sdown + q)
-                    near_over(sdown + q)
+                near_over(sdown + q)
                 diag_over(sdown + q)
 
         def down(i, carry):
@@ -435,9 +461,37 @@
         lax.fori_loop(0, nz // pack, down, 0)
         fin[:, lo:hi] = acc[n % 2, z]
         send_on(n, False)
+        send_late(n - HOLD[0], 0)
+        send_late(n - HOLD[1], 1)
         if n > 0:
             send_on(n - 1, True)
+        if n in starts:
+            p = starts[n] + 1
+            if p < parts:
+                finish(2 + p)
+            if p + 1 < parts:
+                relay(2 + p + 1)
+            for ahead in (p + 3, p + 4) if p == 1 else (p + 4,):
+                if ahead < parts:
+                    first(2 + ahead)
+            if p < parts:
+                near_over(2 + p)
+        if rest == 1 and q + 1 < SPIECES:
+
+            @pl.when(shares)
+            def _():
+                relay(sdown + q + 1)
+
+        if rest == CHUNKS // SPIECES - 1 and q + 1 < SPIECES:
+
+            @pl.when(shares)
+            def _():
+                finish(sdown + q + 1)
+
     send_on(CHUNKS - 1, True)
+    for n in range(CHUNKS, CHUNKS + max(HOLD)):
+        send_late(n - HOLD[0], 0)
+        send_late(n - HOLD[1], 1)
 
     for n in range(CHUNKS):
         lo, hi = n * piece, (n + 1) * piece
@@ -503,7 +557,7 @@
     hbm = pl.BlockSpec(memory_space=pl.ANY)
     return pl.pallas_call(
         functools.partial(kernel, ep, tp, xs, ys, nsh),
-        out_shape=jax.ShapeDtypeStruct((rows, d_model), BF16),
+        out_shape=pltpu.VMEM((rows, d_model), BF16),
         in_specs=[hbm, vm, vm, vm] + [hbm] * 6,
         out_specs=vm,
         scratch_shapes=[

time: 96.6 us -> 88.1 us (0.912)
  Pallas kernels: 94.5 us -> 87.2 us
  local copies, waits for them, and re-layouts: 1.88 us -> 0.8 us
    pallas_call x1, Pallas kernels: 94.5 us -> 87.2 us  [body(): pl.pallas_call(functools.partial(kernel, ep, tp, xs, ys, nsh), out_shape=...]
    unnamed x1, local copies, waits for them, and re-layouts: 1.88 us -> 0.8 us
where the time goes in v3:
time: 88.1 us; the launch traced here: 88 us
  Pallas kernels  87.2 us (99%)
    pallas_call x1, Pallas kernels, body(): pl.pallas_call(functools.partial(kernel, ep, tp, xs, ys, nsh), out_shape=...  87.2 us

profile of v3, /device:TPU:0, one launch (start us, length us, event | category | flops | bytes accessed | tf_op | source)
XLA Modules:
  0.0 88.0 jit_solution(12930324109746247312)
XLA Ops:
  0.0 87.2 %moe.1 = bf16[128,2048]{1,0:T(8,128)(2,1)S(1)} custom-call(bf16[128,2048]{1,0:T(8,128)(2,1)} %tok_ref.1, f32[1,2048]{1,0:T(1,128)} %bitcast.9, s32[2,128]{1,0:T(2,128)} %bitcast.10, f32[2,128]{1,0:T(2,128)} %bitcast.11, bf16[128,2048]{1,0:T(8,128)(2,1)} %bitcast.6, bf16[128,2048]{1,0:T(8,128)(2,1)} %bitcast.7, bf16[128,2048]{1,0:T(8,128)(2,1)} %bitcast.8, ...), custom_call_target="tpu_custom_call" | custom-call | tf_op jit(solution)/shard_map/moe/pallas_call | solution.py:558
  87.2 0.8 copy.12

commit v4 on v3

--- a/solution.py
+++ b/solution.py
@@ -16,7 +16,7 @@
 CHUNKS = 8
 SPIECES = 2
 REACH = 2
-HOLD = (2, 1)
+HOLD = 3
 PIECES = tuple((n, 1) for n in range(CHUNKS))
 
 
@@ -258,8 +258,9 @@
 
     staged = own_rows % 128 == 0 and len(runs_of(near_slots)) == 1
     pack = math.gcd(nz, 4)
-    low = jnp.maximum(z - REACH, 0)
-    high = jnp.minimum(z + REACH + 1, nz)
+    reach = REACH if staged else nz
+    low = jnp.maximum(z - reach, 0)
+    high = jnp.minimum(z + reach + 1, nz)
     dlo, dhi = min(diag_slots), max(diag_slots) + 1
 
     for h in range(2):
@@ -295,6 +296,15 @@
 
         lax.fori_loop(*span, step, 0)
 
+    def within(run):
+        planes_loop(pairs, 2, run)
+        for span in singles:
+            planes_loop(span, 1, run)
+
+    def outside(run):
+        for span in beyond:
+            planes_loop(span, 1, run)
+
     def near_ffn(p, width):
         ffn(p, width, groups)
 
@@ -310,6 +320,7 @@
         first(5)
         for n in range(1, SPIECES):
             first(sdown + n)
+        first(6)
 
     finish(0)
     if staged:
@@ -319,9 +330,7 @@
         travel(3, 0)
     diag_over(0)
     if staged:
-        planes_loop(pairs, 2, early)
-        for span in singles:
-            planes_loop(span, 1, early)
+        within(early)
     finish(1)
     finish(2)
     if nz > 3:
@@ -329,31 +338,23 @@
     for step in range(4, nz):
         for h in range(2):
             travel(step, h)
-    if staged:
-        for span in beyond:
-            planes_loop(span, 1, near_ffn)
-
     @pl.when(jnp.logical_not(shares))
     def _():
         relay(3)
         first(5)
-
-    if staged:
-        for span in beyond:
-            planes_loop(span, 1, early)
+        first(6)
+
     diag_over(1)
 
-    def late(i, carry):
-        p = i * pack
+    def late(p, width):
         if staged:
-            gate = gbuf[pl.ds(p, pack)].reshape(pack * rows, gbuf.shape[2])
-            val = weighted(gate, project(1, p, pack, dlo, dhi), p, pack)
-            hid[pl.ds(p, pack), :, dlo * 2 * own_rows : dhi * 2 * own_rows] = val
+            gate = gbuf[pl.ds(p, width)].reshape(width * rows, gbuf.shape[2])
+            val = weighted(gate, project(1, p, width, dlo, dhi), p, width)
+            hid[pl.ds(p, width), :, dlo * 2 * own_rows : dhi * 2 * own_rows] = val
         else:
-            ffn(p, pack, [(0, tp)])
-        return carry
-
-    lax.fori_loop(0, nz // pack, late, 0)
+            ffn(p, width, [(0, tp)])
+
+    within(late)
     arrive(wts.at[2, 0, 1 - core], r4.at[1])
     near_over(2)
 
@@ -376,6 +377,7 @@
             return carry
 
         lax.fori_loop(0, nz // pack, shared, 0)
+        relay(4)
 
     def link(n, d, sign, j):
         cols = pl.ds(n * piece, piece)
@@ -387,17 +389,22 @@
 
     def each_link(run):
         for j in range(nz - 1, 0, -1):
-            for sign in (1, -1):
+            for sign in (-1, 1):
                 d = z + sign * j
                 there = (d < nz) if sign > 0 else (d >= 0)
                 depth = z if sign > 0 else nz - 1 - z
                 run(d, sign, j, there, depth)
 
-    def send_on(n, lagged):
+    def send_on(n, lagged, far=None):
         lo, hi = n * piece, (n + 1) * piece
 
         def run(d, sign, j, there, depth):
-            @pl.when(there & ((depth >= 2) if lagged else (depth < 2)))
+            if far is not None and far != (j > reach):
+                return
+
+            waits = (depth >= 1) if j == 1 else (depth >= 2)
+
+            @pl.when(there & (waits if lagged else jnp.logical_not(waits)))
             def _():
                 mine_now = acc[n % 2, d]
 
@@ -410,19 +417,19 @@
                 def _():
                     ring[d, :, lo:hi] = mine_now.astype(BF16)
 
-                if lagged or j > 1:
+                if lagged or j > 1 or n == 0:
                     link(n, d, sign, j).start()
 
         each_link(run)
 
-    def send_late(n, wanted):
-        if not 0 <= n < CHUNKS:
+    def send_late(n):
+        if not 0 < n < CHUNKS:
             return
 
         def run(d, sign, j, there, depth):
             if j == 1:
 
-                @pl.when(there & (depth == wanted))
+                @pl.when(there & (depth == 0))
                 def _():
                     link(n, d, sign, j).start()
 
@@ -441,37 +448,55 @@
                 near_over(sdown + q)
                 diag_over(sdown + q)
 
-        def down(i, carry):
-            left = hid[pl.ds(i * pack, pack)].reshape(pack * rows, 2 * tp * own_rows)
+        def down(p, width):
+            left = hid[pl.ds(p, width)].reshape(width * rows, 2 * tp * own_rows)
             right = wts[2, :, :, :, lo:hi].reshape(2 * tp * own_rows, piece)
             o = jnp.dot(left, right, preferred_element_type=F32)
-            acc[n % 2, pl.ds(i * pack, pack)] = o.reshape(pack, rows, piece)
+            acc[n % 2, pl.ds(p, width)] = o.reshape(width, rows, piece)
 
             @pl.when(shares)
             def _():
                 more = jnp.dot(
-                    shid[pl.ds(i * pack, pack)].reshape(pack * rows, 2 * tp * srows),
+                    shid[pl.ds(p, width)].reshape(width * rows, 2 * tp * srows),
                     swts[2, :, :, :, lo:hi].reshape(2 * tp * srows, piece),
                     preferred_element_type=F32,
                 )
-                acc[n % 2, pl.ds(i * pack, pack)] += more.reshape(pack, rows, piece)
-
-            return carry
-
-        lax.fori_loop(0, nz // pack, down, 0)
-        fin[:, lo:hi] = acc[n % 2, z]
-        send_on(n, False)
-        send_late(n - HOLD[0], 0)
-        send_late(n - HOLD[1], 1)
+                acc[n % 2, pl.ds(p, width)] += more.reshape(width, rows, piece)
+
+        if n == 0 and staged:
+            within(down)
+            fin[:, lo:hi] = acc[n % 2, z]
+            send_on(n, False, False)
+
+            @pl.when(jnp.logical_not(shares))
+            def _():
+                outside(near_ffn)
+                relay(4)
+
+            outside(early)
+            outside(late)
+            outside(down)
+            send_on(n, False, True)
+        else:
+            if n == 0:
+
+                @pl.when(jnp.logical_not(shares))
+                def _():
+                    relay(4)
+
+            planes_loop((0, nz // pack), pack, down)
+            fin[:, lo:hi] = acc[n % 2, z]
+            send_on(n, False)
+        send_late(n - HOLD)
         if n > 0:
             send_on(n - 1, True)
         if n in starts:
             p = starts[n] + 1
             if p < parts:
                 finish(2 + p)
-            if p + 1 < parts:
-                relay(2 + p + 1)
-            for ahead in (p + 3, p + 4) if p == 1 else (p + 4,):
+            if p + 2 < parts:
+                relay(2 + p + 2)
+            for ahead in (p + 4, p + 5) if p == 1 else (p + 5,):
                 if ahead < parts:
                     first(2 + ahead)
             if p < parts:
@@ -489,9 +514,8 @@
                 finish(sdown + q + 1)
 
     send_on(CHUNKS - 1, True)
-    for n in range(CHUNKS, CHUNKS + max(HOLD)):
-        send_late(n - HOLD[0], 0)
-        send_late(n - HOLD[1], 1)
+    for n in range(CHUNKS, CHUNKS + HOLD):
+        send_late(n - HOLD)
 
     for n in range(CHUNKS):
         lo, hi = n * piece, (n + 1) * piece

time: 88.1 us -> 87.3 us (level)
  Pallas kernels: 87.2 us -> 86.3 us
    pallas_call x1, Pallas kernels: 87.2 us -> 86.3 us  [body(): pl.pallas_call(functools.partial(kernel, ep, tp, xs, ys, nsh), out_shape=...]
where the time goes in v4:
time: 87.3 us; the launch traced here: 87.1 us
  Pallas kernels  86.3 us (99%)
    pallas_call x1, Pallas kernels, body(): pl.pallas_call(functools.partial(kernel, ep, tp, xs, ys, nsh), out_shape=...  86.3 us

profile of v4, /device:TPU:0, one launch (start us, length us, event | category | flops | bytes accessed | tf_op | source)
XLA Modules:
  0.0 87.1 jit_solution(6097652866157727874)
XLA Ops:
  0.0 86.3 %moe.1 = bf16[128,2048]{1,0:T(8,128)(2,1)S(1)} custom-call(bf16[128,2048]{1,0:T(8,128)(2,1)} %tok_ref.1, f32[1,2048]{1,0:T(1,128)} %bitcast.9, s32[2,128]{1,0:T(2,128)} %bitcast.10, f32[2,128]{1,0:T(2,128)} %bitcast.11, bf16[128,2048]{1,0:T(8,128)(2,1)} %bitcast.6, bf16[128,2048]{1,0:T(8,128)(2,1)} %bitcast.7, bf16[128,2048]{1,0:T(8,128)(2,1)} %bitcast.8, ...), custom_call_target="tpu_custom_call" | custom-call | tf_op jit(solution)/shard_map/moe/pallas_call | solution.py:582
  86.3 0.8 copy.12
